TPU v7x, 32 devices: a whole 2x2x4 slice. The times are simulated.
32 devices in a mesh: fs: 16 (over z, y, core), tp: 2 (over x).
Axes of the slice: x: 2, y: 2, z: 4, core: 2. Of those that a mesh axis runs over, the one named last changes fastest.
Arguments:
- prompt: bfloat16 [2048, 2048], P('fs'), may hold values from -6 to 6
- norm_gain: float32 [2048], P('fs'), may hold values from 0.1 to 1.9
- gate_train: float32 [2048, 32768], P('fs', 'tp'), may hold values from -0.125 to 0.125
- up_train: float32 [2048, 32768], P('fs', 'tp'), may hold values from -0.125 to 0.125
- down_train: float32 [2048, 32768], P('fs', 'tp'), may hold values from -0.25 to 0.25
- common_gate_train: float32 [2048, 512], P('fs', 'tp'), may hold values from -0.125 to 0.125
- common_up_train: float32 [2048, 512], P('fs', 'tp'), may hold values from -0.125 to 0.125
- common_down_train: float32 [2048, 512], P('fs', 'tp'), may hold values from -0.25 to 0.25
- route_ids: int32 [2048, 6], P('fs'), may hold values from 0 to 63, all different within a row; in each aligned block of 128 rows (0 to 127, 128 to 255, ...) at most 16 rows name the same one
- route_weights: float32 [2048, 6], P('fs'), may hold values from 0.1 to 1
Outputs:
- mixture: bfloat16 [2048, 2048], P('fs', 'tp')
- gate_serve: bfloat16 [64, 512, 2048], P('fs', 'tp')
- up_serve: bfloat16 [64, 512, 2048], P('fs', 'tp')
- down_serve: bfloat16 [64, 512, 2048], P('fs', 'tp')
- common_gate_serve: bfloat16 [512, 2048], P('tp')
- common_up_serve: bfloat16 [512, 2048], P('tp')
- common_down_serve: bfloat16 [512, 2048], P('tp')
Inputs may be any that keep to these rules, and one draw needn't show every extreme that they name: `route_ids`: each row names 6 different experts. Among the rows of one index of fs no expert is named more than 16 times, and in every draw some expert is named exactly 16 times by the rows of some index.
All inputs are finite; a program needn't handle non-finite values.
Results may differ from a plain program's by a relative error of at most 0.011.
Values may be sent and summed in bfloat16 or wider, within the bound.
A program may use at most 128 MiB of HBM per device.

v0:
```python
import jax
import jax.numpy as jnp
from jax import lax
from jax.sharding import PartitionSpec as P

FF = 512
E = 64
TOP_K = 6
CAP = 16
epsilon = 1e-06


def shortened(x):
    return jax.tree.map(lambda a: a.astype(jnp.bfloat16) if a.dtype == jnp.float32 else a, x)


def local(
    prompt,
    norm_gain,
    gate_train,
    up_train,
    down_train,
    common_gate_train,
    common_up_train,
    common_down_train,
    route_ids,
    route_weights,
):
    tp_count = lax.axis_size("tp")
    fs_count = lax.axis_size("fs")
    width_rows = gate_train.shape[0]
    local_experts_tp = gate_train.shape[1] // FF
    unit_block = FF // tp_count
    gain_col = norm_gain[:, None]

    def arrange(low):
        sectioned = low.reshape(width_rows, local_experts_tp, tp_count, unit_block)
        sectioned = jnp.transpose(sectioned, (2, 1, 3, 0))
        return sectioned.reshape(tp_count, local_experts_tp, unit_block * width_rows)

    crossed = (
        lax.all_to_all(
            arrange((gate_train * gain_col).astype(jnp.bfloat16)),
            "tp",
            split_axis=0,
            concat_axis=1,
            tiled=True,
        ),
        lax.all_to_all(
            arrange((up_train * gain_col).astype(jnp.bfloat16)),
            "tp",
            split_axis=0,
            concat_axis=1,
            tiled=True,
        ),
        lax.all_to_all(
            arrange(down_train.astype(jnp.bfloat16)), "tp", split_axis=0, concat_axis=1, tiled=True
        ),
    )
    all_experts = crossed[0].shape[1]
    spread = lax.all_to_all(
        shortened(
            tuple((item.reshape(all_experts, 1, unit_block * width_rows) for item in crossed))
        ),
        "fs",
        split_axis=0,
        concat_axis=1,
        tiled=True,
    )

    def finish(arrived_weights):
        owned = arrived_weights.shape[0]
        sectioned = arrived_weights.reshape(owned, fs_count, unit_block, width_rows)
        return jnp.transpose(sectioned, (0, 2, 1, 3)).reshape(
            owned, unit_block, fs_count * width_rows
        )

    gate_serve, up_serve, down_serve = (finish(item) for item in spread)
    common_block = common_gate_train.shape[1]
    common_low = jnp.stack(
        [
            jnp.transpose(common_gate_train * gain_col),
            jnp.transpose(common_up_train * gain_col),
            jnp.transpose(common_down_train),
        ]
    ).astype(jnp.bfloat16)
    common_all = lax.all_gather(
        common_low.reshape(1, 3 * common_block * width_rows), "fs", axis=0, tiled=True
    )
    common_all = jnp.transpose(
        common_all.reshape(fs_count, 3, common_block, width_rows), (1, 2, 0, 3)
    )
    common_all = common_all.reshape(3, common_block, fs_count * width_rows)
    common_gate_serve, common_up_serve, common_down_serve = (
        common_all[0],
        common_all[1],
        common_all[2],
    )
    values = prompt.astype(jnp.float32)
    normed = (
        values * lax.rsqrt(jnp.mean(values * values, axis=1, keepdims=True) + epsilon)
    ).astype(jnp.bfloat16)
    flat_ids = route_ids.reshape(-1)
    onehot = (flat_ids[:, None] == jnp.arange(E, dtype=jnp.int32)[None, :]).astype(jnp.int32)
    before = jnp.cumsum(onehot, axis=0) - onehot
    slot_of = jnp.sum(before * onehot, axis=1)
    target = flat_ids * CAP + slot_of
    model_width = normed.shape[1]
    buffer = (
        jnp.zeros((E * CAP, model_width), jnp.bfloat16)
        .at[target]
        .set(jnp.repeat(normed, TOP_K, axis=0))
    )
    buffer = buffer.reshape(E, CAP, model_width)
    common_gate = jnp.einsum(
        "td,fd->tf", normed, common_gate_serve, preferred_element_type=jnp.float32
    )
    common_up = jnp.einsum("td,fd->tf", normed, common_up_serve, preferred_element_type=jnp.float32)
    common_hidden = (jax.nn.silu(common_gate) * common_up).astype(jnp.bfloat16)
    common_partial = jnp.dot(
        common_hidden, common_down_serve, preferred_element_type=jnp.float32
    ).astype(jnp.bfloat16)
    whole_gate, whole_up, whole_down = (
        lax.all_gather(gate_serve, "tp", axis=1, tiled=True),
        lax.all_gather(up_serve, "tp", axis=1, tiled=True),
        lax.all_gather(down_serve, "tp", axis=1, tiled=True),
    )
    share = CAP // tp_count
    first_slot = lax.axis_index("tp") * share
    my_slots = lax.dynamic_slice_in_dim(buffer, first_slot, share, 1)
    arrived = lax.all_to_all(my_slots, "fs", split_axis=0, concat_axis=1, tiled=True)
    gate_value = jnp.einsum("erd,efd->erf", arrived, whole_gate, preferred_element_type=jnp.float32)
    up_value = jnp.einsum("erd,efd->erf", arrived, whole_up, preferred_element_type=jnp.float32)
    hidden = (jax.nn.silu(gate_value) * up_value).astype(jnp.bfloat16)
    owned, slot_rows = (hidden.shape[0], hidden.shape[1])
    blocked_hidden = hidden.reshape(owned, slot_rows, tp_count, unit_block)
    blocked_down = whole_down.reshape(owned, tp_count, unit_block, model_width)
    partial_value = jnp.einsum(
        "ermf,emfd->merd", blocked_hidden, blocked_down, preferred_element_type=jnp.float32
    ).astype(jnp.bfloat16)
    expert_out = jnp.sum(partial_value.astype(jnp.float32), axis=0).astype(jnp.bfloat16)
    returned = lax.all_to_all(expert_out, "fs", split_axis=1, concat_axis=0, tiled=True)
    inside = (slot_of >= first_slot) & (slot_of < first_slot + share)
    local_index = jnp.where(inside, flat_ids * share + slot_of - first_slot, 0)
    picked = returned.reshape(E * share, model_width)[local_index].astype(jnp.float32)
    pair_weights = jnp.where(inside, route_weights.reshape(-1), 0.0)
    weighted_part = jnp.sum(
        (picked * pair_weights[:, None]).reshape(-1, TOP_K, model_width), axis=1
    )
    weighted, common_sum = (
        lax.psum_scatter(weighted_part, "tp", scatter_dimension=1, tiled=True),
        lax.psum_scatter(common_partial.astype(jnp.float32), "tp", scatter_dimension=1, tiled=True),
    )
    common_out = common_sum.astype(jnp.bfloat16)
    mixture = (weighted + common_out.astype(jnp.float32)).astype(jnp.bfloat16)
    return (
        mixture,
        gate_serve,
        up_serve,
        down_serve,
        common_gate_serve,
        common_up_serve,
        common_down_serve,
    )


def solution(mesh):
    in_specs = (
        P("fs", None),
        P("fs"),
        P("fs", "tp"),
        P("fs", "tp"),
        P("fs", "tp"),
        P("fs", "tp"),
        P("fs", "tp"),
        P("fs", "tp"),
        P("fs", None),
        P("fs", None),
    )
    out_specs = (
        P("fs", "tp"),
        P("fs", "tp", None),
        P("fs", "tp", None),
        P("fs", "tp", None),
        P("tp", None),
        P("tp", None),
        P("tp", None),
    )
    return jax.shard_map(local, mesh=mesh, in_specs=in_specs, out_specs=out_specs, check_vma=False)
```

profile of v0, /device:TPU:0, one launch (start us, length us, event | category | flops | bytes accessed | tf_op | source)
XLA Modules:
  0.0 861.1 jit_solution(5667237024494821347)
XLA Ops:
  7.2 10.8 %multiply_convert_fusion.1 = (bf16[128,16384]{1,0:T(8,128)(2,1)}, bf16[128,16384]{1,0:T(8,128)(2,1)}) fusion(f32[128,16384]{1,0:T(8,128)} %param.12, f32[128]{0:T(128)} %param.11, f32[128,16384]{1,0:T(8,128)} %param.13), kind=kLoop, calls=%fused_computation.6 | loop fusion | flops 8388608 | bytes 25166336 | tf_op jit(solution)/shard_map/convert_element_type | solution.py:43
  25.7 11.3 %copy.100 = bf16[128,32,2,256]{0,3,1,2:T(8,128)(2,1)} copy(bf16[128,32,2,256]{3,2,1,0:T(2,128)(2,1)} %reshape.235) | data formatting | bytes 8388608 | tf_op jit(solution)/shard_map/reshape | solution.py:37
  63.7 11.3 %copy.108 = bf16[128,32,2,256]{0,3,1,2:T(8,128)(2,1)} copy(bf16[128,32,2,256]{3,2,1,0:T(2,128)(2,1)} %reshape.246) | data formatting | bytes 8388608 | tf_op jit(solution)/shard_map/reshape | solution.py:37
  82.2 16.6 %all-to-all-done.1 = bf16[2,32,32768]{2,1,0:T(8,128)(2,1)} async-done(((bf16[2,32,32768]{2,1,0:T(8,128)(2,1)}), bf16[2,32,32768]{2,1,0:T(8,128)(2,1)}, u32[]{:S(2)}, u32[]{:S(2)}) %all-to-all-start.1) | async-done | bytes 4194336 | tf_op jit(solution)/shard_map/all_to_all | solution.py:42
  104.4 7.8 reshape.240
  112.2 11.3 %copy.104 = bf16[128,32,2,256]{0,3,1,2:T(8,128)(2,1)} copy(bf16[128,32,2,256]{3,2,1,0:T(2,128)(2,1)} %reshape.240) | data formatting | bytes 8388608 | tf_op jit(solution)/shard_map/reshape | solution.py:37
  130.8 20.7 %all-to-all-done.5 = bf16[2,32,32768]{2,1,0:T(8,128)(2,1)} async-done(((bf16[2,32,32768]{2,1,0:T(8,128)(2,1)}), bf16[2,32,32768]{2,1,0:T(8,128)(2,1)}, u32[]{:S(2)}, u32[]{:S(2)}) %all-to-all-start.5) | async-done | bytes 4194336 | tf_op jit(solution)/shard_map/all_to_all | solution.py:56
  164.5 7.8 reshape.287
  172.3 31.1 %all-to-all-done.3 = bf16[2,32,32768]{2,1,0:T(8,128)(2,1)} async-done(((bf16[2,32,32768]{2,1,0:T(8,128)(2,1)}), bf16[2,32,32768]{2,1,0:T(8,128)(2,1)}, u32[]{:S(2)}, u32[]{:S(2)}) %all-to-all-start.3) | async-done | bytes 4194336 | tf_op jit(solution)/shard_map/all_to_all | solution.py:49
  215.9 7.9 reshape.291
  223.8 62.9 %all-to-all-done.6 = bf16[16,2,65536]{2,1,0:T(2,128)(2,1)} async-done(((bf16[16,2,65536]{2,1,0:T(2,128)(2,1)}), bf16[16,2,65536]{2,1,0:T(2,128)(2,1)}, u32[]{:S(2)}, u32[]{:S(2)}) %all-to-all-start.6) | async-done | bytes 4194336 | tf_op jit(solution)/shard_map/all_to_all | solution.py:61
  286.7 19.7 %all-to-all-start.2 = ((bf16[16,2,65536]{2,1,0:T(2,128)(2,1)}), bf16[16,2,65536]{2,1,0:T(2,128)(2,1)}, u32[]{:S(2)}, u32[]{:S(2)}) async-start(bf16[16,2,65536]{2,1,0:T(2,128)(2,1)} %reshape.291), calls=%async_computation.2 | async-start | bytes 8388608 | tf_op jit(solution)/shard_map/all_to_all | solution.py:61
  306.6 12.3 %reshape.288 = bf16[64,1,32768]{2,1,0:T(2,128)(2,1)} reshape(bf16[16,2,65536]{2,1,0:T(2,128)(2,1)} %all-to-all-done.6) | data formatting | bytes 8388608
  318.9 26.1 %reduce.5 = bf16[64,32768]{1,0:T(8,128)(2,1)} reduce(bf16[64,1,32768]{2,1,0:T(2,128)(2,1)} %reshape.288, bf16[]{:T(256)} %constant.38), dimensions={1}, to_apply=%all_to_all.91.reduce_sub_computation | reduce | bytes 8388610 | tf_op jit(solution)/shard_map/all_to_all | solution.py:61
  352.2 8.4 reshape.277
  373.6 8.3 reshape.289
  383.9 19.7 %all-to-all-start.4 = ((bf16[16,2,65536]{2,1,0:T(2,128)(2,1)}), bf16[16,2,65536]{2,1,0:T(2,128)(2,1)}, u32[]{:S(2)}, u32[]{:S(2)}) async-start(bf16[16,2,65536]{2,1,0:T(2,128)(2,1)} %reshape.289), calls=%async_computation.4 | async-start | bytes 8388608 | tf_op jit(solution)/shard_map/all_to_all | solution.py:61
  403.7 12.4 %reshape.292 = bf16[64,1,32768]{2,1,0:T(2,128)(2,1)} reshape(bf16[16,2,65536]{2,1,0:T(2,128)(2,1)} %all-to-all-done.2) | data formatting | bytes 8388608
  416.1 26.1 %reduce.3 = bf16[64,32768]{1,0:T(8,128)(2,1)} reduce(bf16[64,1,32768]{2,1,0:T(2,128)(2,1)} %reshape.292, bf16[]{:T(256)} %constant.38), dimensions={1}, to_apply=%all_to_all.83.reduce_sub_computation | reduce | bytes 8388610 | tf_op jit(solution)/shard_map/all_to_all | solution.py:61
  449.3 8.4 reshape.275
  462.9 18.3 %all-to-all-done.4 = bf16[16,2,65536]{2,1,0:T(2,128)(2,1)} async-done(((bf16[16,2,65536]{2,1,0:T(2,128)(2,1)}), bf16[16,2,65536]{2,1,0:T(2,128)(2,1)}, u32[]{:S(2)}, u32[]{:S(2)}) %all-to-all-start.4) | async-done | bytes 4194336 | tf_op jit(solution)/shard_map/all_to_all | solution.py:61
  481.2 12.7 %reshape.290 = bf16[64,1,32768]{2,1,0:T(2,128)(2,1)} reshape(bf16[16,2,65536]{2,1,0:T(2,128)(2,1)} %all-to-all-done.4) | data formatting | bytes 8388608
  493.9 26.1 %reduce.4 = bf16[64,32768]{1,0:T(8,128)(2,1)} reduce(bf16[64,1,32768]{2,1,0:T(2,128)(2,1)} %reshape.290, bf16[]{:T(256)} %constant.38), dimensions={1}, to_apply=%all_to_all.87.reduce_sub_computation | reduce | bytes 8388610 | tf_op jit(solution)/shard_map/all_to_all | solution.py:61
  527.1 8.4 reshape.276
  553.0 9.4 %scatter_custom_fusion = bf16[1024,2048]{1,0:T(8,128)(2,1)} fusion(s32[768]{0:T(1024)S(1)} %get-tuple-element.29, bf16[768,2048]{1,0:T(8,128)(2,1)S(1)} %reshape.267, bf16[]{:T(256)} %constant.11.clone.1), kind=kCustom, calls=%fused_computation.17 | custom fusion | bytes 4194306 | tf_op jit(solution)/shard_map/scatter | solution.py:112
  565.6 19.3 %all-to-all-start = ((bf16[64,8,2048]{2,1,0:T(8,128)(2,1)}), bf16[64,8,2048]{2,1,0:T(8,128)(2,1)S(1)}, u32[]{:S(2)}, u32[]{:S(2)}) async-start(bf16[64,8,2048]{2,1,0:T(8,128)(2,1)} %constant_dynamic-slice_fusion), calls=%async_computation | async-start | bytes 4194304 | tf_op jit(solution)/shard_map/all_to_all | solution.py:131
  586.6 12.0 %copy.112 = bf16[4,512,2048]{2,1,0:T(8,128)(2,1)} copy(bf16[4,512,2048]{1,2,0:T(8,128)(2,1)} %all-gather.10.cloned.1.call-done) | data formatting | bytes 16777216 | tf_op jit(solution)/shard_map/all_gather | solution.py:126
  598.6 27.3 %all-to-all-done = bf16[64,8,2048]{2,1,0:T(8,128)(2,1)S(1)} async-done(((bf16[64,8,2048]{2,1,0:T(8,128)(2,1)}), bf16[64,8,2048]{2,1,0:T(8,128)(2,1)S(1)}, u32[]{:S(2)}, u32[]{:S(2)}) %all-to-all-start) | async-done | bytes 2097184 | tf_op jit(solution)/shard_map/all_to_all | solution.py:131
  632.2 51.4 %all-gather.8.cloned.1.call-done = bf16[4,512,2048]{2,1,0:T(8,128)(2,1)} async-done(((bf16[4,256,2048]{2,1,0:T(8,128)(2,1)}), bf16[4,512,2048]{2,1,0:T(8,128)(2,1)}) %all-gather.8.cloned.1.call-update) | async-done | bytes 8388624 | tf_op jit(solution)/shard_map/all_gather | solution.py:125
  700.3 79.5 %all-gather.12.cloned.1.call-done = bf16[16,1,98304]{2,1,0:T(2,128)(2,1)} async-done(((bf16[1,1,98304]{2,1,0:T(2,128)(2,1)}), bf16[16,1,98304]{2,1,0:T(2,128)(2,1)}) %all-gather.12.cloned.1.call-update) | async-done | bytes 3145744 | tf_op jit(solution)/shard_map/all_gather | solution.py:87
  779.8 18.5 %reduce.7 = bf16[16,98304]{1,0:T(8,128)(2,1)S(1)} reduce(bf16[16,1,98304]{2,1,0:T(2,128)(2,1)} %all-gather.12.cloned.1.call-done, bf16[]{:T(256)} %constant.38), dimensions={1}, to_apply=%all-gather.reduce_sub_computation | reduce | bytes 6291458 | tf_op jit(solution)/shard_map/all_gather | solution.py:87
  840.0 12.1 %reduce-scatter.3.cloned.1.call-done = f32[128,1024]{1,0:T(8,128)} async-done(((f32[128,2048]{1,0:T(8,128)}), f32[128,1024]{1,0:T(8,128)}) %reduce-scatter.3.cloned.1.call-update) | async-done | bytes 524304 | tf_op jit(solution)/shard_map/reduce_scatter | solution.py:151
  (114 shorter events, 210.6 us)
Async XLA Ops:
  44.4 54.5 %all-to-all-start.1 = ((bf16[2,32,32768]{2,1,0:T(8,128)(2,1)}), bf16[2,32,32768]{2,1,0:T(8,128)(2,1)}, u32[]{:S(2)}, u32[]{:S(2)}) async-start(bf16[2,32,32768]{2,1,0:T(8,128)(2,1)} %reshape.236), calls=%async_computation.1 | async-start | bytes 8388608 | tf_op jit(solution)/shard_map/all_to_all | solution.py:42
  98.8 52.7 %all-to-all-start.5 = ((bf16[2,32,32768]{2,1,0:T(8,128)(2,1)}), bf16[2,32,32768]{2,1,0:T(8,128)(2,1)}, u32[]{:S(2)}, u32[]{:S(2)}) async-start(bf16[2,32,32768]{2,1,0:T(8,128)(2,1)} %reshape.247), calls=%async_computation.5 | async-start | bytes 8388608 | tf_op jit(solution)/shard_map/all_to_all | solution.py:56
  151.5 51.9 %all-to-all-start.3 = ((bf16[2,32,32768]{2,1,0:T(8,128)(2,1)}), bf16[2,32,32768]{2,1,0:T(8,128)(2,1)}, u32[]{:S(2)}, u32[]{:S(2)}) async-start(bf16[2,32,32768]{2,1,0:T(8,128)(2,1)} %reshape.241), calls=%async_computation.3 | async-start | bytes 8388608 | tf_op jit(solution)/shard_map/all_to_all | solution.py:49
  203.4 83.3 %all-to-all-start.6 = ((bf16[16,2,65536]{2,1,0:T(2,128)(2,1)}), bf16[16,2,65536]{2,1,0:T(2,128)(2,1)}, u32[]{:S(2)}, u32[]{:S(2)}) async-start(bf16[16,2,65536]{2,1,0:T(2,128)(2,1)} %reshape.287), calls=%async_computation.6 | async-start | bytes 8388608 | tf_op jit(solution)/shard_map/all_to_all | solution.py:61
  286.7 97.2 %all-to-all-start.2 = ((bf16[16,2,65536]{2,1,0:T(2,128)(2,1)}), bf16[16,2,65536]{2,1,0:T(2,128)(2,1)}, u32[]{:S(2)}, u32[]{:S(2)}) async-start(bf16[16,2,65536]{2,1,0:T(2,128)(2,1)} %reshape.291), calls=%async_computation.2 | async-start | bytes 8388608 | tf_op jit(solution)/shard_map/all_to_all | solution.py:61
  306.4 280.2 %all-gather.10.cloned.1.call-start = ((), (), s32[]{:S(2)}) async-start(), calls=%async_computation.12 | async-start | bytes 12582912 | tf_op jit(solution)/shard_map/all_gather | solution.py:126
  383.9 97.2 %all-to-all-start.4 = ((bf16[16,2,65536]{2,1,0:T(2,128)(2,1)}), bf16[16,2,65536]{2,1,0:T(2,128)(2,1)}, u32[]{:S(2)}, u32[]{:S(2)}) async-start(bf16[16,2,65536]{2,1,0:T(2,128)(2,1)} %reshape.289), calls=%async_computation.4 | async-start | bytes 8388608 | tf_op jit(solution)/shard_map/all_to_all | solution.py:61
  403.6 222.3 %all-gather.6.cloned.1.call-start = ((), (), s32[]{:S(2)}) async-start(), calls=%async_computation.10 | async-start | bytes 12582912 | tf_op jit(solution)/shard_map/all_gather | solution.py:124
  462.6 221.0 %all-gather.8.cloned.1.call-start = ((), (), s32[]{:S(2)}) async-start(), calls=%async_computation.11 | async-start | bytes 12582912 | tf_op jit(solution)/shard_map/all_gather | solution.py:125
  540.4 0.7 copy-start.10
  540.4 3.7 copy-start.6
  544.5 0.8 copy-start.5
  562.4 22.9 %copy-start.7 = (f32[128,256]{1,0:T(8,128)S(1)}, f32[128,256]{1,0:T(8,128)}, u32[]{:S(2)}) copy-start(f32[128,256]{1,0:T(8,128)} %param.15) | copy-start | bytes 393220
  562.4 22.9 %copy-start.8 = (f32[128,256]{1,0:T(8,128)S(1)}, f32[128,256]{1,0:T(8,128)}, u32[]{:S(2)}) copy-start(f32[128,256]{1,0:T(8,128)} %param.16) | copy-start | bytes 393220
  562.4 22.9 %copy-start.9 = (f32[128,256]{1,0:T(8,128)S(1)}, f32[128,256]{1,0:T(8,128)}, u32[]{:S(2)}) copy-start(f32[128,256]{1,0:T(8,128)} %param.17) | copy-start | bytes 393220
  562.4 23.0 %copy-start.12 = (f32[128]{0:T(128)S(1)}, f32[128]{0:T(128)}, u32[]{:S(2)}) copy-start(f32[128]{0:T(128)} %param.11) | copy-start | bytes 1540
  565.6 60.3 %all-to-all-start = ((bf16[64,8,2048]{2,1,0:T(8,128)(2,1)}), bf16[64,8,2048]{2,1,0:T(8,128)(2,1)S(1)}, u32[]{:S(2)}, u32[]{:S(2)}) async-start(bf16[64,8,2048]{2,1,0:T(8,128)(2,1)} %constant_dynamic-slice_fusion), calls=%async_computation | async-start | bytes 4194304 | tf_op jit(solution)/shard_map/all_to_all | solution.py:131
  584.9 194.8 %all-gather.12.cloned.1.call-start = ((), (), s32[]{:S(2)}) async-start(), calls=%async_computation.15 | async-start | bytes 6684672 | tf_op jit(solution)/shard_map/all_gather | solution.py:87
  683.6 6.5 copy-start.4
  694.4 113.8 %all-to-all-start.7 = ((bf16[4,128,2048]{2,0,1:T(4,128)(2,1)}), bf16[4,128,2048]{2,0,1:T(4,128)(2,1)}, u32[]{:S(2)}, u32[]{:S(2)}) async-start(bf16[4,128,2048]{2,0,1:T(4,128)(2,1)} %copy.115), calls=%async_computation.7 | async-start | bytes 4194304 | tf_op jit(solution)/shard_map/all_to_all | solution.py:142
  700.1 140.0 %reduce-scatter.5.cloned.1.call-start = ((), (), s32[]{:S(2)}) async-start(), calls=%async_computation.14 | async-start | bytes 1572864 | tf_op jit(solution)/shard_map/reduce_scatter | solution.py:152
  801.1 6.7 copy-start
  801.1 6.9 copy-start.11
  803.0 7.9 copy-start.2
  807.8 44.3 %reduce-scatter.3.cloned.1.call-start = ((), (), s32[]{:S(2)}) async-start(), calls=%async_computation.13 | async-start | bytes 1572864 | tf_op jit(solution)/shard_map/reduce_scatter | solution.py:151
  821.9 9.1 %copy-start.1 = (bf16[1,256,16,128]{1,3,2,0:T(8,128)(2,1)S(1)}, bf16[1,256,16,128]{1,3,2,0:T(8,128)(2,1)}, u32[]{:S(2)}) copy-start(bf16[1,256,16,128]{1,3,2,0:T(8,128)(2,1)} %copy-done) | copy-start | bytes 3145732
  829.5 2.9 copy-start.3
Sparse Core Ops, SparseCore 0:
  367.0 104.2 all-gather.9
  473.4 103.9 all-gather.5
  579.5 103.9 all-gather.7
  686.3 93.4 all-gather.11
  807.9 21.5 reduce-scatter.4
  831.6 20.3 reduce-scatter.2
where the time goes:
time: 875 us; the launch traced here: 861 us
  waiting for transfers between devices  322 us (37%)
  local copies, waits for them, and re-layouts  271 us (31%)
  other arithmetic  146 us (17%)
  starting transfers between devices  88.1 us (10%)
  matrix products  18.9 us (2%)
  between operations  14.7 us (2%)
    all_to_all x3, waiting for transfers between devices, local(): lax.all_to_all(shortened(tuple((item.reshape(all_experts, 1, unit_block *...  83.2 us
    all_gather x1, waiting for transfers between devices, local(): lax.all_gather(common_low.reshape(1, 3 * common_block * width_rows), 'fs'...  79.5 us
    all_to_all x3, other arithmetic, local(): lax.all_to_all(shortened(tuple((item.reshape(all_experts, 1, unit_block *...  78.3 us
    unnamed x40, local copies, waits for them, and re-layouts  75 us
    reshape x6, local copies, waits for them, and re-layouts, arrange(): sectioned = low.reshape(width_rows, local_experts_tp, tp_count, unit_block)  57.2 us
    all_gather x1, waiting for transfers between devices, local(): lax.all_gather(up_serve, 'tp', axis=1, tiled=True)  51.4 us
    all_to_all x3, starting transfers between devices, local(): lax.all_to_all(shortened(tuple((item.reshape(all_experts, 1, unit_block *...  45.1 us
    all_to_all x1, waiting for transfers between devices, local(): lax.all_to_all(arrange((up_train * gain_col).astype(jnp.bfloat16)), 'tp',...  31.1 us
  transfers between devices with their start and end apart: 14, of which 10 were waited for; matrix products, arithmetic and copies ran while one was open for 43% of the time, Pallas kernels for 0%

commit v1 on v0

--- a/solution.py
+++ b/solution.py
@@ -120,9 +120,14 @@
     common_partial = jnp.dot(
         common_hidden, common_down_serve, preferred_element_type=jnp.float32
     ).astype(jnp.bfloat16)
+
+    def begin_patches_on(inp):
+        wide_out = jnp.concatenate(lax.all_gather(inp, "tp"), 1)
+        return wide_out
+
     whole_gate, whole_up, whole_down = (
         lax.all_gather(gate_serve, "tp", axis=1, tiled=True),
-        lax.all_gather(up_serve, "tp", axis=1, tiled=True),
+        begin_patches_on(up_serve),
         lax.all_gather(down_serve, "tp", axis=1, tiled=True),
     )
     share = CAP // tp_count

time: 875 us -> 901 us (1.030)
  local copies, waits for them, and re-layouts: 271 us -> 293 us
    all_gather x1, waiting for transfers between devices: 51.4 us -> 0.02 us  [begin_patches_on(): wide_out = jnp.concatenate(lax.all_gather(inp, 'tp'), 1)]
    all_gather x1, waiting for transfers between devices: 0.01 us -> 50 us  [local(): lax.all_gather(gate_serve, 'tp', axis=1, tiled=True)]
    all_to_all x3, waiting for transfers between devices: 83.2 us -> 131 us  [local(): lax.all_to_all(shortened(tuple((item.reshape(all_experts, 1, unit_block *...]
    all_to_all x1, waiting for transfers between devices: 16.6 us -> 0.01 us  [local(): lax.all_to_all(arrange((gate_train * gain_col).astype(jnp.bfloat16)), 'tp...]
    all_to_all x1, waiting for transfers between devices: 31.1 us -> 16.6 us  [local(): lax.all_to_all(arrange((up_train * gain_col).astype(jnp.bfloat16)), 'tp',...]
    all_to_all x1, waiting for transfers between devices: 20.7 us -> 31.9 us  [local(): lax.all_to_all(arrange(down_train.astype(jnp.bfloat16)), 'tp', split_axis...]
    unnamed x40 -> x45, local copies, waits for them, and re-layouts: 75 us -> 80.4 us
  transfers between devices with their start and end apart: 14 -> 14, of which waited for: 10 -> 9; matrix products, arithmetic and copies ran while one was open for 43% -> 44% of each run, Pallas kernels for 0% -> 0%
where the time goes in v1:
time: 901 us; the launch traced here: 889 us
  waiting for transfers between devices  331 us (37%)
  local copies, waits for them, and re-layouts  293 us (33%)
  other arithmetic  146 us (16%)
  starting transfers between devices  89 us (10%)
  matrix products  15.7 us (2%)
  between operations  14.7 us (2%)
    all_to_all x3, waiting for transfers between devices, local(): lax.all_to_all(shortened(tuple((item.reshape(all_experts, 1, unit_block *...  131 us
    unnamed x45, local copies, waits for them, and re-layouts  80.4 us
    all_to_all x3, other arithmetic, local(): lax.all_to_all(shortened(tuple((item.reshape(all_experts, 1, unit_block *...  78.3 us
    all_gather x1, waiting for transfers between devices, local(): lax.all_gather(common_low.reshape(1, 3 * common_block * width_rows), 'fs'...  76.2 us
    reshape x6, local copies, waits for them, and re-layouts, arrange(): sectioned = low.reshape(width_rows, local_experts_tp, tp_count, unit_block)  57.2 us
    all_gather x1, waiting for transfers between devices, local(): lax.all_gather(gate_serve, 'tp', axis=1, tiled=True)  50 us
    all_to_all x3, starting transfers between devices, local(): lax.all_to_all(shortened(tuple((item.reshape(all_experts, 1, unit_block *...  45.8 us
    all_to_all x1, waiting for transfers between devices, local(): lax.all_to_all(arrange(down_train.astype(jnp.bfloat16)), 'tp', split_axis...  31.9 us
  transfers between devices with their start and end apart: 14, of which 9 were waited for; matrix products, arithmetic and copies ran while one was open for 44% of the time, Pallas kernels for 0%

profile of v1, /device:TPU:0, one launch (start us, length us, event | category | flops | bytes accessed | tf_op | source)
XLA Modules:
  0.0 888.9 jit_solution(17843416166543938858)
XLA Ops:
  7.2 10.8 %multiply_convert_fusion.1 = (bf16[128,16384]{1,0:T(8,128)(2,1)}, bf16[128,16384]{1,0:T(8,128)(2,1)}) fusion(f32[128,16384]{1,0:T(8,128)} %param.12, f32[128]{0:T(128)} %param.11, f32[128,16384]{1,0:T(8,128)} %param.13), kind=kLoop, calls=%fused_computation.6 | loop fusion | flops 8388608 | bytes 25166336 | tf_op jit(solution)/shard_map/convert_element_type | solution.py:43
  25.7 11.3 %copy.110 = bf16[128,32,2,256]{0,3,1,2:T(8,128)(2,1)} copy(bf16[128,32,2,256]{3,2,1,0:T(2,128)(2,1)} %reshape.246) | data formatting | bytes 8388608 | tf_op jit(solution)/shard_map/reshape | solution.py:37
  63.7 11.3 %copy.116 = bf16[128,32,2,256]{0,3,1,2:T(8,128)(2,1)} copy(bf16[128,32,2,256]{3,2,1,0:T(2,128)(2,1)} %reshape.253) | data formatting | bytes 8388608 | tf_op jit(solution)/shard_map/reshape | solution.py:37
  82.2 16.6 %all-to-all-done.3 = bf16[2,32,32768]{2,1,0:T(8,128)(2,1)} async-done(((bf16[2,32,32768]{2,1,0:T(8,128)(2,1)}), bf16[2,32,32768]{2,1,0:T(8,128)(2,1)}, u32[]{:S(2)}, u32[]{:S(2)}) %all-to-all-start.3) | async-done | bytes 4194336 | tf_op jit(solution)/shard_map/all_to_all | solution.py:49
  111.8 7.9 reshape.297
  119.6 31.9 %all-to-all-done.5 = bf16[2,32,32768]{2,1,0:T(8,128)(2,1)} async-done(((bf16[2,32,32768]{2,1,0:T(8,128)(2,1)}), bf16[2,32,32768]{2,1,0:T(8,128)(2,1)}, u32[]{:S(2)}, u32[]{:S(2)}) %all-to-all-start.5) | async-done | bytes 4194336 | tf_op jit(solution)/shard_map/all_to_all | solution.py:56
  157.5 7.8 reshape.241
  165.3 11.3 %copy.106 = bf16[128,32,2,256]{0,3,1,2:T(8,128)(2,1)} copy(bf16[128,32,2,256]{3,2,1,0:T(2,128)(2,1)} %reshape.241) | data formatting | bytes 8388608 | tf_op jit(solution)/shard_map/reshape | solution.py:37
  183.9 51.2 %all-to-all-done.4 = bf16[16,2,65536]{2,1,0:T(2,128)(2,1)} async-done(((bf16[16,2,65536]{2,1,0:T(2,128)(2,1)}), bf16[16,2,65536]{2,1,0:T(2,128)(2,1)}, u32[]{:S(2)}, u32[]{:S(2)}) %all-to-all-start.4) | async-done | bytes 4194336 | tf_op jit(solution)/shard_map/all_to_all | solution.py:61
  240.9 12.3 %reshape.298 = bf16[64,1,32768]{2,1,0:T(2,128)(2,1)} reshape(bf16[16,2,65536]{2,1,0:T(2,128)(2,1)} %all-to-all-done.4) | data formatting | bytes 8388608
  253.2 26.1 %reduce.4 = bf16[64,32768]{1,0:T(8,128)(2,1)} reduce(bf16[64,1,32768]{2,1,0:T(2,128)(2,1)} %reshape.298, bf16[]{:T(256)} %constant.38), dimensions={1}, to_apply=%all_to_all.87.reduce_sub_computation | reduce | bytes 8388610 | tf_op jit(solution)/shard_map/all_to_all | solution.py:61
  286.5 8.4 reshape.284
  314.2 7.8 reshape.295
  322.0 20.1 %all-to-all-start.6 = ((bf16[16,2,65536]{2,1,0:T(2,128)(2,1)}), bf16[16,2,65536]{2,1,0:T(2,128)(2,1)}, u32[]{:S(2)}, u32[]{:S(2)}) async-start(bf16[16,2,65536]{2,1,0:T(2,128)(2,1)} %reshape.295), calls=%async_computation.6 | async-start | bytes 8388608 | tf_op jit(solution)/shard_map/all_to_all | solution.py:61
  348.9 7.8 reshape.299
  356.8 62.9 %all-to-all-done.6 = bf16[16,2,65536]{2,1,0:T(2,128)(2,1)} async-done(((bf16[16,2,65536]{2,1,0:T(2,128)(2,1)}), bf16[16,2,65536]{2,1,0:T(2,128)(2,1)}, u32[]{:S(2)}, u32[]{:S(2)}) %all-to-all-start.6) | async-done | bytes 4194336 | tf_op jit(solution)/shard_map/all_to_all | solution.py:61
  419.7 19.7 %all-to-all-start.2 = ((bf16[16,2,65536]{2,1,0:T(2,128)(2,1)}), bf16[16,2,65536]{2,1,0:T(2,128)(2,1)}, u32[]{:S(2)}, u32[]{:S(2)}) async-start(bf16[16,2,65536]{2,1,0:T(2,128)(2,1)} %reshape.299), calls=%async_computation.2 | async-start | bytes 8388608 | tf_op jit(solution)/shard_map/all_to_all | solution.py:61
  439.4 12.4 %reshape.296 = bf16[64,1,32768]{2,1,0:T(2,128)(2,1)} reshape(bf16[16,2,65536]{2,1,0:T(2,128)(2,1)} %all-to-all-done.6) | data formatting | bytes 8388608
  451.8 26.1 %reduce.5 = bf16[64,32768]{1,0:T(8,128)(2,1)} reduce(bf16[64,1,32768]{2,1,0:T(2,128)(2,1)} %reshape.296, bf16[]{:T(256)} %constant.38), dimensions={1}, to_apply=%all_to_all.91.reduce_sub_computation | reduce | bytes 8388610 | tf_op jit(solution)/shard_map/all_to_all | solution.py:61
  485.1 8.4 reshape.285
  499.9 17.0 %all-to-all-done.2 = bf16[16,2,65536]{2,1,0:T(2,128)(2,1)} async-done(((bf16[16,2,65536]{2,1,0:T(2,128)(2,1)}), bf16[16,2,65536]{2,1,0:T(2,128)(2,1)}, u32[]{:S(2)}, u32[]{:S(2)}) %all-to-all-start.2) | async-done | bytes 4194336 | tf_op jit(solution)/shard_map/all_to_all | solution.py:61
  516.9 12.4 %reshape.300 = bf16[64,1,32768]{2,1,0:T(2,128)(2,1)} reshape(bf16[16,2,65536]{2,1,0:T(2,128)(2,1)} %all-to-all-done.2) | data formatting | bytes 8388608
  529.3 26.1 %reduce.3 = bf16[64,32768]{1,0:T(8,128)(2,1)} reduce(bf16[64,1,32768]{2,1,0:T(2,128)(2,1)} %reshape.300, bf16[]{:T(256)} %constant.38), dimensions={1}, to_apply=%all_to_all.83.reduce_sub_computation | reduce | bytes 8388610 | tf_op jit(solution)/shard_map/all_to_all | solution.py:61
  562.6 8.4 reshape.283
  588.5 9.4 %scatter_custom_fusion = bf16[1024,2048]{1,0:T(8,128)(2,1)} fusion(s32[768]{0:T(1024)S(1)} %get-tuple-element.29, bf16[768,2048]{1,0:T(8,128)(2,1)S(1)} %reshape.275, bf16[]{:T(256)} %constant.11.clone.1), kind=kCustom, calls=%fused_computation.16 | custom fusion | bytes 4194306 | tf_op jit(solution)/shard_map/scatter | solution.py:112
  601.1 19.6 %all-to-all-start = ((bf16[64,8,2048]{2,1,0:T(8,128)(2,1)}), bf16[64,8,2048]{2,1,0:T(8,128)(2,1)S(1)}, u32[]{:S(2)}, u32[]{:S(2)}) async-start(bf16[64,8,2048]{2,1,0:T(8,128)(2,1)} %constant_dynamic-slice_fusion), calls=%async_computation | async-start | bytes 4194304 | tf_op jit(solution)/shard_map/all_to_all | solution.py:136
  622.4 9.0 %copy.115 = bf16[4,2,256,2048]{3,2,1,0:T(8,128)(2,1)} copy(bf16[4,2,256,2048]{3,2,0,1:T(8,128)(2,1)} %bitcast.131) | data formatting | bytes 16777216 | tf_op jit(solution)/shard_map/reshape | solution.py:125
  631.4 11.4 %copy.120 = bf16[4,512,2048]{2,1,0:T(8,128)(2,1)} copy(bf16[4,512,2048]{1,2,0:T(8,128)(2,1)} %all-gather.10.cloned.1.call-done) | data formatting | bytes 16777216 | tf_op jit(solution)/shard_map/all_gather | solution.py:131
  642.8 18.9 %all-to-all-done = bf16[64,8,2048]{2,1,0:T(8,128)(2,1)S(1)} async-done(((bf16[64,8,2048]{2,1,0:T(8,128)(2,1)}), bf16[64,8,2048]{2,1,0:T(8,128)(2,1)S(1)}, u32[]{:S(2)}, u32[]{:S(2)}) %all-to-all-start) | async-done | bytes 2097184 | tf_op jit(solution)/shard_map/all_to_all | solution.py:136
  661.7 50.0 %all-gather.6.cloned.1.call-done = bf16[4,512,2048]{2,1,0:T(8,128)(2,1)} async-done(((bf16[4,256,2048]{2,1,0:T(8,128)(2,1)}), bf16[4,512,2048]{2,1,0:T(8,128)(2,1)}) %all-gather.6.cloned.1.call-update) | async-done | bytes 8388624 | tf_op jit(solution)/shard_map/all_gather | solution.py:129
  731.5 76.2 %all-gather.12.cloned.1.call-done = bf16[16,1,98304]{2,1,0:T(2,128)(2,1)} async-done(((bf16[1,1,98304]{2,1,0:T(2,128)(2,1)}), bf16[16,1,98304]{2,1,0:T(2,128)(2,1)}) %all-gather.12.cloned.1.call-update) | async-done | bytes 3145744 | tf_op jit(solution)/shard_map/all_gather | solution.py:87
  807.7 18.5 %reduce.7 = bf16[16,98304]{1,0:T(8,128)(2,1)S(1)} reduce(bf16[16,1,98304]{2,1,0:T(2,128)(2,1)} %all-gather.12.cloned.1.call-done, bf16[]{:T(256)} %constant.38), dimensions={1}, to_apply=%all-gather.reduce_sub_computation | reduce | bytes 6291458 | tf_op jit(solution)/shard_map/all_gather | solution.py:87
  (122 shorter events, 225.1 us)
Async XLA Ops:
  44.4 54.5 %all-to-all-start.3 = ((bf16[2,32,32768]{2,1,0:T(8,128)(2,1)}), bf16[2,32,32768]{2,1,0:T(8,128)(2,1)}, u32[]{:S(2)}, u32[]{:S(2)}) async-start(bf16[2,32,32768]{2,1,0:T(8,128)(2,1)} %reshape.247), calls=%async_computation.3 | async-start | bytes 8388608 | tf_op jit(solution)/shard_map/all_to_all | solution.py:49
  98.8 52.7 %all-to-all-start.5 = ((bf16[2,32,32768]{2,1,0:T(8,128)(2,1)}), bf16[2,32,32768]{2,1,0:T(8,128)(2,1)}, u32[]{:S(2)}, u32[]{:S(2)}) async-start(bf16[2,32,32768]{2,1,0:T(8,128)(2,1)} %reshape.254), calls=%async_computation.5 | async-start | bytes 8388608 | tf_op jit(solution)/shard_map/all_to_all | solution.py:56
  151.5 83.5 %all-to-all-start.4 = ((bf16[16,2,65536]{2,1,0:T(2,128)(2,1)}), bf16[16,2,65536]{2,1,0:T(2,128)(2,1)}, u32[]{:S(2)}, u32[]{:S(2)}) async-start(bf16[16,2,65536]{2,1,0:T(2,128)(2,1)} %reshape.297), calls=%async_computation.4 | async-start | bytes 8388608 | tf_op jit(solution)/shard_map/all_to_all | solution.py:61
  235.1 86.9 %all-to-all-start.1 = ((bf16[2,32,32768]{2,1,0:T(8,128)(2,1)}), bf16[2,32,32768]{2,1,0:T(8,128)(2,1)}, u32[]{:S(2)}, u32[]{:S(2)}) async-start(bf16[2,32,32768]{2,1,0:T(8,128)(2,1)} %reshape.242), calls=%async_computation.1 | async-start | bytes 8388608 | tf_op jit(solution)/shard_map/all_to_all | solution.py:42
  240.7 381.7 %all-gather.8.cloned.1.call-start = ((), (), s32[]{:S(2)}) async-start(), calls=%async_computation.11 | async-start | bytes 12582912 | tf_op jit(solution)/shard_map/all_gather | solution.py:125
  322.0 97.6 %all-to-all-start.6 = ((bf16[16,2,65536]{2,1,0:T(2,128)(2,1)}), bf16[16,2,65536]{2,1,0:T(2,128)(2,1)}, u32[]{:S(2)}, u32[]{:S(2)}) async-start(bf16[16,2,65536]{2,1,0:T(2,128)(2,1)} %reshape.295), calls=%async_computation.6 | async-start | bytes 8388608 | tf_op jit(solution)/shard_map/all_to_all | solution.py:61
  419.7 97.2 %all-to-all-start.2 = ((bf16[16,2,65536]{2,1,0:T(2,128)(2,1)}), bf16[16,2,65536]{2,1,0:T(2,128)(2,1)}, u32[]{:S(2)}, u32[]{:S(2)}) async-start(bf16[16,2,65536]{2,1,0:T(2,128)(2,1)} %reshape.299), calls=%async_computation.2 | async-start | bytes 8388608 | tf_op jit(solution)/shard_map/all_to_all | solution.py:61
  439.4 192.0 %all-gather.10.cloned.1.call-start = ((), (), s32[]{:S(2)}) async-start(), calls=%async_computation.12 | async-start | bytes 12582912 | tf_op jit(solution)/shard_map/all_gather | solution.py:131
  499.7 212.0 %all-gather.6.cloned.1.call-start = ((), (), s32[]{:S(2)}) async-start(), calls=%async_computation.10 | async-start | bytes 12582912 | tf_op jit(solution)/shard_map/all_gather | solution.py:129
  575.8 0.7 copy-start.10
  575.8 3.7 copy-start.6
  579.9 0.8 copy-start.5
  597.9 23.2 %copy-start.7 = (f32[128,256]{1,0:T(8,128)S(1)}, f32[128,256]{1,0:T(8,128)}, u32[]{:S(2)}) copy-start(f32[128,256]{1,0:T(8,128)} %param.15) | copy-start | bytes 393220
  597.9 23.2 %copy-start.8 = (f32[128,256]{1,0:T(8,128)S(1)}, f32[128,256]{1,0:T(8,128)}, u32[]{:S(2)}) copy-start(f32[128,256]{1,0:T(8,128)} %param.16) | copy-start | bytes 393220
  597.9 23.2 %copy-start.9 = (f32[128,256]{1,0:T(8,128)S(1)}, f32[128,256]{1,0:T(8,128)}, u32[]{:S(2)}) copy-start(f32[128,256]{1,0:T(8,128)} %param.17) | copy-start | bytes 393220
  597.9 23.3 %copy-start.12 = (f32[128]{0:T(128)S(1)}, f32[128]{0:T(128)}, u32[]{:S(2)}) copy-start(f32[128]{0:T(128)} %param.11) | copy-start | bytes 1540
  601.1 60.6 %all-to-all-start = ((bf16[64,8,2048]{2,1,0:T(8,128)(2,1)}), bf16[64,8,2048]{2,1,0:T(8,128)(2,1)S(1)}, u32[]{:S(2)}, u32[]{:S(2)}) async-start(bf16[64,8,2048]{2,1,0:T(8,128)(2,1)} %constant_dynamic-slice_fusion), calls=%async_computation | async-start | bytes 4194304 | tf_op jit(solution)/shard_map/all_to_all | solution.py:136
  620.7 187.0 %all-gather.12.cloned.1.call-start = ((), (), s32[]{:S(2)}) async-start(), calls=%async_computation.15 | async-start | bytes 6684672 | tf_op jit(solution)/shard_map/all_gather | solution.py:87
  711.7 6.5 copy-start.4
  711.7 9.6 %slice-start = ((s8[8388608]{0:T(1024)(128)(4,1)}), s8[4194304]{0:T(1024)(128)(4,1)S(1)}, s32[]{:S(2)}) async-start(s8[8388608]{0:T(1024)(128)(4,1)} %bitcast.133), calls=%async_computation.16 | async-start | bytes 8388608
  718.1 3.1 slice-start.1
  725.6 110.5 %all-to-all-start.7 = ((bf16[4,128,2048]{2,0,1:T(4,128)(2,1)}), bf16[4,128,2048]{2,0,1:T(4,128)(2,1)}, u32[]{:S(2)}, u32[]{:S(2)}) async-start(bf16[4,128,2048]{2,0,1:T(4,128)(2,1)} %copy.123), calls=%async_computation.7 | async-start | bytes 4194304 | tf_op jit(solution)/shard_map/all_to_all | solution.py:147
  731.3 142.9 %reduce-scatter.5.cloned.1.call-start = ((), (), s32[]{:S(2)}) async-start(), calls=%async_computation.14 | async-start | bytes 1572864 | tf_op jit(solution)/shard_map/reduce_scatter | solution.py:157
  829.1 6.7 copy-start
  829.1 6.9 copy-start.11
  831.0 7.9 copy-start.2
  835.8 44.2 %reduce-scatter.3.cloned.1.call-start = ((), (), s32[]{:S(2)}) async-start(), calls=%async_computation.13 | async-start | bytes 1572864 | tf_op jit(solution)/shard_map/reduce_scatter | solution.py:156
  849.9 9.1 %copy-start.1 = (bf16[1,256,16,128]{1,3,2,0:T(8,128)(2,1)S(1)}, bf16[1,256,16,128]{1,3,2,0:T(8,128)(2,1)}, u32[]{:S(2)}) copy-start(bf16[1,256,16,128]{1,3,2,0:T(8,128)(2,1)} %copy-done) | copy-start | bytes 3145732
  857.5 2.9 copy-start.3
Sparse Core Ops, SparseCore 0:
  307.5 119.3 all-gather.7
  499.8 105.6 all-gather.9
  607.6 103.9 all-gather.5
  714.4 93.3 all-gather.11
  835.9 21.4 reduce-scatter.4
  859.5 20.3 reduce-scatter.2
